TPU v7x, 32 devices: a whole 2x2x4 slice. The times are simulated.
32 devices in a mesh: ep: 8 (over z, core), tp: 4 (over y, x).
Axes of the slice: x: 2, y: 2, z: 4, core: 2. Of those that a mesh axis runs over, the one named last changes fastest.
Arguments:
- q_latent: bfloat16 [1536, 512], P('ep'), may hold values from -6 to 6
- kv_latent: bfloat16 [1536, 256], P('ep'), may hold values from -6 to 6
- rope_key: bfloat16 [1536, 64], P('ep'), may hold values from -900 to 900
- q_gain: float32 [512], replicated, may hold values from 0.1 to 1.9
- kv_gain: float32 [256], replicated, may hold values from 0.1 to 1.9
- w_query: bfloat16 [512, 3072], P(None, 'tp'), may hold values from -0.25 to 0.25
- w_key: bfloat16 [256, 2048], P(None, 'tp'), may hold values from -0.375 to 0.375
- w_value: bfloat16 [256, 2048], P(None, 'tp'), may hold values from -0.375 to 0.375
- w_mix_out: bfloat16 [2048, 2048], P('tp'), may hold values from -0.125 to 0.125
- expert_in: bfloat16 [1024, 2048], P('ep'), may hold values from -6 to 6
- norm_gain: float32 [2048], replicated, may hold values from 0.1 to 1.9
- routes: int32 [1024, 2], P('ep'), may hold values from 0 to 7, all different within a row; in each aligned block of 128 rows (0 to 127, 128 to 255, ...) at most 64 rows name the same one
- route_scores: float32 [1024, 2], P('ep'), may hold values from 0.05 to 1
- w_gate: bfloat16 [8, 2048, 4096], P('ep', None, 'tp'), may hold values from -0.125 to 0.125
- w_up: bfloat16 [8, 2048, 4096], P('ep', None, 'tp'), may hold values from -0.125 to 0.125
- w_down: bfloat16 [8, 4096, 2048], P('ep', 'tp'), may hold values from -0.125 to 0.125
Outputs:
- mixed: bfloat16 [1536, 2048], P(('ep', 'tp'))
- expert_out: bfloat16 [1024, 2048], P('ep', 'tp')
Inputs may be any that keep to these rules, and one draw needn't show every extreme that they name: `routes`: each row names 2 different experts; in the rows of one index of ep no expert is named by more than 64 rows, a bound that some block reaches.
All inputs are finite; a program needn't handle non-finite values.
Results may differ from a plain program's by a relative error of at most 0.03.
The roundings to bfloat16 on the way count: a program that leaves them out, or rounds other values in their place, can miss the bound.
Values may be sent and summed in bfloat16 or wider, within the bound.
No kernel may reach another device: no remote copies, remote signals or barrier semaphores. Data moves between devices by JAX's collectives and lax.ppermute only.
A program may use at most 64 MiB of HBM per device.

v0:
```python
import jax
import jax.numpy as jnp
from jax import lax
from jax.sharding import PartitionSpec as P

NOPE = 128
ROPE = 64
VDIM = 128
eps_norm = 1e-05
rope_base = 10000.0


def rms_scale(values, gain):
    wide = values.astype(jnp.float32)
    return wide * lax.rsqrt(jnp.mean(wide * wide, -1, keepdims=True) + eps_norm) * gain


def rotate(values, cosine, sine):
    first, second = jnp.split(values, 2, axis=-1)
    return jnp.concatenate([first * cosine - second * sine, first * sine + second * cosine], -1)


def angles(positions):
    inverse = rope_base ** (-jnp.arange(0, ROPE, 2).astype(jnp.float32) / ROPE)
    phase = positions[:, None] * inverse[None, :]
    return (jnp.cos(phase), jnp.sin(phase))


def mixer(q_latent, kv_latent, rope_key, q_gain, kv_gain, w_query, w_key, w_value, w_mix_out):
    token_count = q_latent.shape[0]
    head_count = w_key.shape[1] // NOPE
    offset = lax.axis_index("ep") * token_count
    positions = (offset + jnp.arange(token_count, dtype=jnp.int32)).astype(jnp.float32)
    cosine, sine = angles(positions)
    q_normed = rms_scale(q_latent, q_gain).astype(jnp.bfloat16)
    kv_normed = rms_scale(kv_latent, kv_gain).astype(jnp.bfloat16)
    key_turned = rotate(rope_key.astype(jnp.float32), cosine, sine).astype(jnp.bfloat16)
    query = jnp.dot(q_normed, w_query, preferred_element_type=jnp.float32).astype(jnp.bfloat16)
    query = query.reshape(token_count, head_count, NOPE + ROPE)
    q_pass = query[:, :, :NOPE]
    q_turned = rotate(
        query[:, :, NOPE:].astype(jnp.float32), cosine[:, None, :], sine[:, None, :]
    ).astype(jnp.bfloat16)
    factor = (NOPE + ROPE) ** (-0.5)
    peak = jnp.full((head_count, token_count), -jnp.inf, jnp.float32)
    total = jnp.zeros((head_count, token_count), jnp.float32)
    summed = jnp.zeros((token_count, head_count, VDIM), jnp.float32)
    latent = lax.all_gather(kv_normed, "ep", axis=0, tiled=True)
    turned = lax.all_gather(key_turned, "ep", axis=0, tiled=True)
    count = latent.shape[0]
    keys = jnp.dot(latent, w_key, preferred_element_type=jnp.float32).astype(jnp.bfloat16)
    keys = keys.reshape(count, head_count, NOPE)
    values = jnp.dot(latent, w_value, preferred_element_type=jnp.float32).astype(jnp.bfloat16)
    values = values.reshape(count, head_count, VDIM)
    scores = jnp.einsum("qhd,khd->hqk", q_pass, keys, preferred_element_type=jnp.float32)
    scores = (
        scores + jnp.einsum("qhd,kd->hqk", q_turned, turned, preferred_element_type=jnp.float32)
    ) * factor
    fresh = jnp.max(scores, -1)
    fade = jnp.exp(peak - fresh)
    weights = jnp.exp(scores - fresh[:, :, None])
    total = total * fade + jnp.sum(weights, -1)
    update = jnp.einsum(
        "hqk,khd->qhd", weights.astype(jnp.bfloat16), values, preferred_element_type=jnp.float32
    )
    summed = summed * jnp.transpose(fade)[:, :, None] + update
    peak, total, summed = (fresh, total, summed)
    attended = (summed / jnp.transpose(total)[:, :, None]).astype(jnp.bfloat16)
    attended = attended.reshape(token_count, head_count * VDIM)
    return lax.psum_scatter(
        jnp.dot(attended, w_mix_out, preferred_element_type=jnp.float32).astype(jnp.bfloat16),
        "tp",
        scatter_dimension=0,
        tiled=True,
    )


def experts(expert_in, norm_gain, routes, route_scores, w_gate, w_up, w_down):
    token_count, width = expert_in.shape
    choose = routes.shape[1]
    expert_count = lax.axis_size("ep")
    slots = 2 * choose * token_count // expert_count
    wide = expert_in.astype(jnp.float32)
    centered = wide - jnp.mean(wide, -1, keepdims=True)
    normed = (
        centered
        * lax.rsqrt(jnp.mean(centered * centered, -1, keepdims=True) + eps_norm)
        * norm_gain
    ).astype(jnp.bfloat16)
    shares = route_scores / jnp.sum(route_scores, -1, keepdims=True)
    flat_expert = routes.reshape(-1)
    onehot = (flat_expert[:, None] == jnp.arange(expert_count, dtype=jnp.int32)[None, :]).astype(
        jnp.int32
    )
    before = jnp.sum((jnp.cumsum(onehot, 0) - onehot) * onehot, 1)
    target = flat_expert * slots + before
    source = jnp.arange(token_count * choose, dtype=jnp.int32) // choose
    table = jnp.full((expert_count * slots,), token_count, jnp.int32).at[target].set(source)
    padded = jnp.concatenate([normed, jnp.zeros((1, width), jnp.bfloat16)], 0)
    outgoing = padded[table].reshape(expert_count, slots, width)
    gate_weight = w_gate[0]
    up_weight = w_up[0]
    down_weight = w_down[0]
    arrived = lax.all_to_all(outgoing, "ep", split_axis=0, concat_axis=0, tiled=True).reshape(
        expert_count * slots, width
    )
    gate = jnp.dot(arrived, gate_weight, preferred_element_type=jnp.float32)
    up = jnp.dot(arrived, up_weight, preferred_element_type=jnp.float32)
    hidden = (jax.nn.silu(gate) * up).astype(jnp.bfloat16)
    summed = lax.psum_scatter(
        lax.dot_general(
            down_weight, hidden, (((0,), (1,)), ((), ())), preferred_element_type=jnp.float32
        ).astype(jnp.bfloat16),
        "tp",
        scatter_dimension=0,
        tiled=True,
    )
    feature_count = summed.shape[0]
    returned = lax.all_to_all(
        summed.reshape(feature_count, expert_count, slots),
        "ep",
        split_axis=1,
        concat_axis=1,
        tiled=True,
    )
    picked = jnp.take(returned.reshape(feature_count, expert_count * slots), target, axis=1)
    picked = picked.reshape(feature_count, token_count, choose).astype(jnp.float32)
    combined = jnp.sum(picked * shares[None, :, :], -1)
    return jnp.transpose(combined).astype(jnp.bfloat16)


def body(
    q_latent,
    kv_latent,
    rope_key,
    q_gain,
    kv_gain,
    w_query,
    w_key,
    w_value,
    w_mix_out,
    expert_in,
    norm_gain,
    routes,
    route_scores,
    w_gate,
    w_up,
    w_down,
):
    mixed = mixer(
        q_latent, kv_latent, rope_key, q_gain, kv_gain, w_query, w_key, w_value, w_mix_out
    )
    expert_out = experts(expert_in, norm_gain, routes, route_scores, w_gate, w_up, w_down)
    return (mixed, expert_out)


def solution(mesh):
    in_specs = (
        P("ep", None),
        P("ep", None),
        P("ep", None),
        P(),
        P(),
        P(None, "tp"),
        P(None, "tp"),
        P(None, "tp"),
        P("tp", None),
        P("ep", None),
        P(),
        P("ep", None),
        P("ep", None),
        P("ep", None, "tp"),
        P("ep", None, "tp"),
        P("ep", "tp", None),
    )
    out_specs = (P(("ep", "tp"), None), P("ep", "tp"))
    return jax.shard_map(body, mesh=mesh, in_specs=in_specs, out_specs=out_specs, check_vma=False)
```

profile of v0, /device:TPU:0, one launch (start us, length us, event | category | flops | bytes accessed | tf_op | source)
XLA Modules:
  0.0 162.9 jit_solution(18064462734204936463)
XLA Ops:
  7.2 0.9 copy.51
  10.3 1.4 scatter_custom_fusion
  11.7 1.2 convert_reduce_fusion
  12.9 1.3 fusion.37
  14.3 1.4 fusion.39
  15.7 3.3 %gather_fusion = bf16[512,2048]{1,0:T(8,128)(2,1)} fusion(bf16[129,2048]{1,0:T(8,128)(2,1)S(1)} %concatenate.13, s32[1024]{0:T(1024)S(1)} %pad_clamp_fusion.1), kind=kCustom, calls=%fused_computation | custom fusion | bytes 4196352 | tf_op jit(solution)/shard_map/gather | solution.py:100
  19.1 6.5 %all-to-all-start = ((bf16[8,64,2048]{2,1,0:T(8,128)(2,1)}), bf16[8,64,2048]{2,1,0:T(8,128)(2,1)}, u32[]{:S(2)}, u32[]{:S(2)}) async-start(bf16[8,64,2048]{2,1,0:T(8,128)(2,1)} %bitcast.82), calls=%async_computation.1 | async-start | bytes 4194304 | tf_op jit(solution)/shard_map/all_to_all | solution.py:104
  26.1 1.5 convolution_convert_fusion.3
  27.6 47.2 %all-to-all-done = bf16[8,64,2048]{2,1,0:T(8,128)(2,1)} async-done(((bf16[8,64,2048]{2,1,0:T(8,128)(2,1)}), bf16[8,64,2048]{2,1,0:T(8,128)(2,1)}, u32[]{:S(2)}, u32[]{:S(2)}) %all-to-all-start) | async-done | bytes 2097184 | tf_op jit(solution)/shard_map/all_to_all | solution.py:104
  74.7 6.5 %fusion.5 = f32[512,1024]{1,0:T(8,128)} fusion(bf16[512,2048]{1,0:T(8,128)(2,1)} %bitcast.12, bf16[1,2048,1024]{2,1,0:T(8,128)(2,1)} %param.29), kind=kOutput, calls=%fused_computation.10 | convolution fusion | flops 2147483648 | bytes 8388608 | tf_op jit(solution)/shard_map/dot_general | solution.py:107
  81.2 10.6 %fusion.12 = bf16[2048,512]{0,1:T(8,128)(2,1)} fusion(bf16[1,1024,2048]{2,1,0:T(8,128)(2,1)} %param.31, f32[512,1024]{1,0:T(8,128)} %fusion.5, bf16[512,2048]{1,0:T(8,128)(2,1)} %bitcast.12, bf16[1,2048,1024]{2,1,0:T(8,128)(2,1)} %param.30), kind=kOutput, calls=%fused_computation.17 | convolution fusion | flops 4299161600 | bytes 14680064 | tf_op jit(solution)/shard_map/dot_general | solution.py:111
  92.5 14.2 %all-gather = bf16[8,192,64]{1,2,0:T(8,128)(2,1)S(1)} all-gather(bf16[1,192,64]{1,2,0:T(8,128)(2,1)S(1)} %maximum_bitcast_fusion), channel_id=1, replica_groups=mesh['ep'=8,'tp'=4] {'ep'}, dimensions={0}, use_global_device_ids=true | all-gather | bytes 221184 | tf_op jit(solution)/shard_map/all_gather | solution.py:49
  107.4 16.3 %all_gather.6 = bf16[1536,256]{1,0:T(8,128)(2,1)S(1)} all-gather(bf16[192,256]{1,0:T(8,128)(2,1)S(1)} %fusion.47), channel_id=1, replica_groups=mesh['ep'=8,'tp'=4] {'ep'}, dimensions={0}, use_global_device_ids=true | all-gather | bytes 884736 | tf_op jit(solution)/shard_map/all_gather | solution.py:48
  123.7 1.6 convolution_convert_fusion.1
  125.3 0.8 fusion.54
  126.2 0.9 fusion.65
  127.1 0.8 fusion.7
  128.7 0.9 fusion.34
  129.6 1.5 convolution_convert_fusion.2
  131.2 3.5 %all-to-all-start.1 = ((bf16[512,8,64]{0,2,1:T(8,128)(2,1)}), bf16[512,8,64]{0,2,1:T(8,128)(2,1)S(1)}, u32[]{:S(2)}, u32[]{:S(2)}) async-start(bf16[512,8,64]{0,2,1:T(8,128)(2,1)} %bitcast.86), calls=%async_computation.3 | async-start | bytes 1048576 | tf_op jit(solution)/shard_map/all_to_all | solution.py:119
  135.2 14.7 %all-to-all-done.1 = bf16[512,8,64]{0,2,1:T(8,128)(2,1)S(1)} async-done(((bf16[512,8,64]{0,2,1:T(8,128)(2,1)}), bf16[512,8,64]{0,2,1:T(8,128)(2,1)S(1)}, u32[]{:S(2)}, u32[]{:S(2)}) %all-to-all-start.1) | async-done | bytes 524320 | tf_op jit(solution)/shard_map/all_to_all | solution.py:119
  149.9 1.2 gather_fusion.1
  151.2 1.5 multiply_reduce_fusion
  152.7 3.4 %reduce-scatter.3.cloned.1.call-done = bf16[48,2048]{1,0:T(8,128)(2,1)} async-done(((bf16[192,2048]{1,0:T(8,128)(2,1)}), bf16[48,2048]{1,0:T(8,128)(2,1)}) %reduce-scatter.3.cloned.1.call-update) | async-done | bytes 196624 | tf_op jit(solution)/shard_map/reduce_scatter | solution.py:70
  (74 shorter events, 5.5 us)
Async XLA Ops:
  7.2 122.4 %copy-start = (bf16[512,2048]{1,0:T(8,128)(2,1)S(1)}, bf16[512,2048]{1,0:T(8,128)(2,1)}, u32[]{:S(2)}) copy-start(bf16[512,2048]{1,0:T(8,128)(2,1)} %param.24) | copy-start | bytes 6291460
  19.1 6.5 %copy-start.5 = (bf16[192,64]{0,1:T(8,128)(2,1)S(1)}, bf16[192,64]{0,1:T(8,128)(2,1)}, u32[]{:S(2)}) copy-start(bf16[192,64]{0,1:T(8,128)(2,1)} %param.18) | copy-start | bytes 73732
  19.1 6.6 %copy-start.2 = (bf16[192,512]{1,0:T(8,128)(2,1)S(1)}, bf16[192,512]{1,0:T(8,128)(2,1)}, u32[]{:S(2)}) copy-start(bf16[192,512]{1,0:T(8,128)(2,1)} %param.16) | copy-start | bytes 589828
  19.1 7.0 %copy-start.8 = (f32[512]{0:T(512)S(1)}, f32[512]{0:T(512)}, u32[]{:S(2)}) copy-start(f32[512]{0:T(512)} %param.19) | copy-start | bytes 6148
  19.1 55.6 %all-to-all-start = ((bf16[8,64,2048]{2,1,0:T(8,128)(2,1)}), bf16[8,64,2048]{2,1,0:T(8,128)(2,1)}, u32[]{:S(2)}, u32[]{:S(2)}) async-start(bf16[8,64,2048]{2,1,0:T(8,128)(2,1)} %bitcast.82), calls=%async_computation.1 | async-start | bytes 4194304 | tf_op jit(solution)/shard_map/all_to_all | solution.py:104
  25.6 105.6 %reduce-scatter.5.cloned.1.call-start = ((), (), s32[]{:S(2)}) async-start(), calls=%async_computation.5 | async-start | bytes 2621440 | tf_op jit(solution)/shard_map/reduce_scatter | solution.py:110
  91.8 15.3 %copy-start.3 = (bf16[192,256]{1,0:T(8,128)(2,1)S(1)}, bf16[192,256]{1,0:T(8,128)(2,1)}, u32[]{:S(2)}) copy-start(bf16[192,256]{1,0:T(8,128)(2,1)} %param.17) | copy-start | bytes 294916
  91.8 15.5 %copy-start.9 = (f32[256]{0:T(256)S(1)}, f32[256]{0:T(256)}, u32[]{:S(2)}) copy-start(f32[256]{0:T(256)} %param.20) | copy-start | bytes 3076
  91.8 64.3 %reduce-scatter.3.cloned.1.call-start = ((), (), s32[]{:S(2)}) async-start(), calls=%async_computation.4 | async-start | bytes 983040 | tf_op jit(solution)/shard_map/reduce_scatter | solution.py:70
  92.3 31.4 %copy-start.1 = (bf16[192,4,192]{2,1,0:T(4,128)(2,1)}, bf16[192,4,192]{2,1,0:T(4,128)(2,1)S(1)}, u32[]{:S(2)}) copy-start(bf16[192,4,192]{2,1,0:T(4,128)(2,1)S(1)} %reshape.186) | copy-start | bytes 884740
  125.3 0.9 slice-start
  127.1 1.0 copy-start.4
  129.6 5.3 %copy-start.6 = (s32[128,2]{0,1:T(2,128)S(1)}, s32[128,2]{0,1:T(2,128)}, u32[]{:S(2)}) copy-start(s32[128,2]{0,1:T(2,128)} %param.27) | copy-start | bytes 3076
  129.6 5.5 %copy-start.7 = (f32[128,2]{0,1:T(2,128)S(1)}, f32[128,2]{0,1:T(2,128)}, u32[]{:S(2)}) copy-start(f32[128,2]{0,1:T(2,128)} %param.28) | copy-start | bytes 3076
  131.2 18.8 %all-to-all-start.1 = ((bf16[512,8,64]{0,2,1:T(8,128)(2,1)}), bf16[512,8,64]{0,2,1:T(8,128)(2,1)S(1)}, u32[]{:S(2)}, u32[]{:S(2)}) async-start(bf16[512,8,64]{0,2,1:T(8,128)(2,1)} %bitcast.86), calls=%async_computation.3 | async-start | bytes 1048576 | tf_op jit(solution)/shard_map/all_to_all | solution.py:119
Sparse Core Ops, SparseCore 0:
  91.9 34.1 reduce-scatter.4
  131.3 24.7 reduce-scatter.2
where the time goes:
time: 164 us; the launch traced here: 163 us
  waiting for transfers between devices  65.3 us (40%)
  blocking collectives  30.5 us (19%)
  matrix products  24.9 us (15%)
  between operations  14.4 us (9%)
  starting transfers between devices  10.1 us (6%)
  local copies, waits for them, and re-layouts  9.44 us (6%)
  other arithmetic  8.38 us (5%)
    all_to_all x1, waiting for transfers between devices, experts(): lax.all_to_all(outgoing, 'ep', split_axis=0, concat_axis=0, tiled=True)  47.2 us
    all_gather x1, blocking collectives, mixer(): latent = lax.all_gather(kv_normed, 'ep', axis=0, tiled=True)  16.3 us
    all_to_all x1, waiting for transfers between devices, experts(): lax.all_to_all(summed.reshape(feature_count, expert_count, slots), 'ep',...  14.7 us
    all_gather x1, blocking collectives, mixer(): turned = lax.all_gather(key_turned, 'ep', axis=0, tiled=True)  14.2 us
    dot_general x1, matrix products, experts(): lax.dot_general(down_weight, hidden, (((0,), (1,)), ((), ())), preferred_...  10.6 us
    all_to_all x1, starting transfers between devices, experts(): lax.all_to_all(outgoing, 'ep', split_axis=0, concat_axis=0, tiled=True)  6.49 us
    dot_general x1, matrix products, experts(): gate = jnp.dot(arrived, gate_weight, preferred_element_type=jnp.float32)  6.48 us
    all_to_all x1, starting transfers between devices, experts(): lax.all_to_all(summed.reshape(feature_count, expert_count, slots), 'ep',...  3.5 us
  transfers between devices with their start and end apart: 4, of which 3 were waited for; matrix products, arithmetic and copies ran while one was open for 8% of the time, Pallas kernels for 0%

commit v1 on v0

--- a/solution.py
+++ b/solution.py
@@ -8,6 +8,33 @@
 VDIM = 128
 eps_norm = 1e-05
 rope_base = 10000.0
+
+
+def open_the_row(w_in, original):
+    block_now, right_arr, current_value = (
+        jax.lax.axis_size("ep"),
+        jax.lax.axis_index("ep"),
+        w_in.shape[0],
+    )
+    h_now, frame_out = ([], [])
+    near = z_new = w_in
+    for dev_i in range(block_now // 2 + 1):
+        h_now.append(original(near, (right_arr - dev_i) % block_now * current_value))
+        if 0 < dev_i < block_now - block_now // 2:
+            frame_out.append(original(z_new, (right_arr + dev_i) % block_now * current_value))
+        near = jax.lax.ppermute(
+            near,
+            axis_name="ep",
+            perm=[(dev_j, (dev_j + 1) % block_now) for dev_j in range(block_now)],
+        )
+        z_new = jax.lax.ppermute(
+            z_new, "ep", perm=[(dev_j, (dev_j - 1) % block_now) for dev_j in range(block_now)]
+        )
+    return jnp.roll(
+        jnp.concatenate([*h_now[::-1], *frame_out], 2),
+        shift=(right_arr - block_now // 2) * h_now[0].shape[2],
+        axis=2,
+    )
 
 
 def rms_scale(values, gain):
@@ -46,7 +73,6 @@
     total = jnp.zeros((head_count, token_count), jnp.float32)
     summed = jnp.zeros((token_count, head_count, VDIM), jnp.float32)
     latent = lax.all_gather(kv_normed, "ep", axis=0, tiled=True)
-    turned = lax.all_gather(key_turned, "ep", axis=0, tiled=True)
     count = latent.shape[0]
     keys = jnp.dot(latent, w_key, preferred_element_type=jnp.float32).astype(jnp.bfloat16)
     keys = keys.reshape(count, head_count, NOPE)
@@ -54,7 +80,13 @@
     values = values.reshape(count, head_count, VDIM)
     scores = jnp.einsum("qhd,khd->hqk", q_pass, keys, preferred_element_type=jnp.float32)
     scores = (
-        scores + jnp.einsum("qhd,kd->hqk", q_turned, turned, preferred_element_type=jnp.float32)
+        scores
+        + open_the_row(
+            key_turned,
+            original=lambda own_block, start: jnp.einsum(
+                "qhd,kd->hqk", q_turned, own_block, preferred_element_type=jnp.float32
+            ),
+        )
     ) * factor
     fresh = jnp.max(scores, -1)
     fade = jnp.exp(peak - fresh)

time: 164 us -> 183 us (1.12)
  waiting for transfers between devices: 65.3 us -> 20.7 us
  blocking collectives: 30.5 us -> 52.1 us
  matrix products: 24.9 us -> 40 us
  local copies, waits for them, and re-layouts: 9.44 us -> 22.7 us
  starting transfers between devices: 10.1 us -> 20.8 us
  other arithmetic: 8.38 us -> 11.3 us
    all_to_all x1, waiting for transfers between devices: 47.2 us -> 0.01 us  [experts(): lax.all_to_all(outgoing, 'ep', split_axis=0, concat_axis=0, tiled=True)]
    all_gather x1, blocking collectives: 16.3 us -> 52.1 us  [mixer(): latent = lax.all_gather(kv_normed, 'ep', axis=0, tiled=True)]
    all_gather x1 -> x0, blocking collectives: 14.2 us -> none  [mixer(): turned = lax.all_gather(key_turned, 'ep', axis=0, tiled=True)]
    concatenate x0 -> x1, local copies, waits for them, and re-layouts: none -> 12.7 us  [open_the_row(): jnp.roll(jnp.concatenate([*h_now[::-1], *frame_out], 2), shift=(right_arr...]
    ppermute x0 -> x7, starting transfers between devices: none -> 10.7 us  [the longest x3 9.79 us: open_the_row(): jax.lax.ppermute(z_new, 'ep', perm=[(dev_j, (dev_j - 1) % block_now) for...]
    dot_general x1 -> x8, matrix products: 0.81 us -> 10.3 us  [mixer(): jnp.einsum('qhd,kd->hqk', q_turned, own_block, preferred_element_type=jnp...]
    dot_general x1, matrix products: 0.87 us -> 4.44 us  [mixer(): jnp.einsum('qhd,khd->hqk', q_pass, keys, preferred_element_type=jnp.float32)]
    ppermute x0 -> x7, waiting for transfers between devices: none -> 2.72 us  [the longest x4 2.71 us: open_the_row(): jax.lax.ppermute(near, axis_name='ep', perm=[(dev_j, (dev_j + 1) % block_...]
  transfers between devices with their start and end apart: 4 -> 11, of which waited for: 3 -> 3; matrix products, arithmetic and copies ran while one was open for 8% -> 33% of each run, Pallas kernels for 0% -> 0%
where the time goes in v1:
time: 183 us; the launch traced here: 182 us
  blocking collectives  52.1 us (28%)
  matrix products  40 us (22%)
  local copies, waits for them, and re-layouts  22.7 us (12%)
  starting transfers between devices  20.8 us (11%)
  waiting for transfers between devices  20.7 us (11%)
  between operations  14.4 us (8%)
  other arithmetic  11.3 us (6%)
    all_gather x1, blocking collectives, mixer(): latent = lax.all_gather(kv_normed, 'ep', axis=0, tiled=True)  52.1 us
    all_to_all x1, waiting for transfers between devices, experts(): lax.all_to_all(summed.reshape(feature_count, expert_count, slots), 'ep',...  14.7 us
    concatenate x1, local copies, waits for them, and re-layouts, open_the_row(): jnp.roll(jnp.concatenate([*h_now[::-1], *frame_out], 2), shift=(right_arr...  12.7 us
    dot_general x1, matrix products, experts(): lax.dot_general(down_weight, hidden, (((0,), (1,)), ((), ())), preferred_...  10.5 us
    dot_general x8, matrix products, mixer(): jnp.einsum('qhd,kd->hqk', q_turned, own_block, preferred_element_type=jnp...  10.3 us
    ppermute x3, starting transfers between devices, open_the_row(): jax.lax.ppermute(z_new, 'ep', perm=[(dev_j, (dev_j - 1) % block_now) for...  9.79 us
    all_to_all x1, starting transfers between devices, experts(): lax.all_to_all(outgoing, 'ep', split_axis=0, concat_axis=0, tiled=True)  6.5 us
    dot_general x1, matrix products, experts(): gate = jnp.dot(arrived, gate_weight, preferred_element_type=jnp.float32)  6.45 us
  transfers between devices with their start and end apart: 11, of which 3 were waited for; matrix products, arithmetic and copies ran while one was open for 33% of the time, Pallas kernels for 0%

profile of v1, /device:TPU:0, one launch (start us, length us, event | category | flops | bytes accessed | tf_op | source)
XLA Modules:
  0.0 182.0 jit_solution(10498332403360430557)
XLA Ops:
  10.3 1.4 scatter_custom_fusion
  12.9 1.3 fusion.36
  14.3 1.4 fusion.38
  15.7 3.3 %gather_fusion = bf16[512,2048]{1,0:T(8,128)(2,1)} fusion(bf16[129,2048]{1,0:T(8,128)(2,1)S(1)} %concatenate.20, s32[1024]{0:T(1024)S(1)} %pad_clamp_fusion.1), kind=kCustom, calls=%fused_computation | custom fusion | bytes 4196352 | tf_op jit(solution)/shard_map/gather | solution.py:132
  19.0 6.5 %all-to-all-start = ((bf16[8,64,2048]{2,1,0:T(8,128)(2,1)}), bf16[8,64,2048]{2,1,0:T(8,128)(2,1)}, u32[]{:S(2)}, u32[]{:S(2)}) async-start(bf16[8,64,2048]{2,1,0:T(8,128)(2,1)} %bitcast.113), calls=%async_computation.1 | async-start | bytes 4194304 | tf_op jit(solution)/shard_map/all_to_all | solution.py:136
  27.6 3.1 %collective-permute-start.4 = (bf16[192,64]{0,1:T(8,128)(2,1)}, bf16[192,64]{0,1:T(8,128)(2,1)}, u32[]{:S(2)}, u32[]{:S(2)}) collective-permute-start(bf16[192,64]{0,1:T(8,128)(2,1)} %pad_maximum_fusion.1), channel_id=1, source_target_pairs={{0,28},{4,0},{8,4},{12,8},{16,12},{20,16},{24,20},{28,24},{1,29},{... | collective-permute-start | bytes 73736 | tf_op jit(solution)/shard_map/ppermute | solution.py:30
  32.7 52.1 %all_gather.3 = bf16[1536,256]{1,0:T(8,128)(2,1)S(1)} all-gather(bf16[192,256]{1,0:T(8,128)(2,1)S(1)} %fusion.46), channel_id=1, replica_groups=mesh['ep'=8,'tp'=4] {'ep'}, dimensions={0}, use_global_device_ids=true | all-gather | bytes 884736 | tf_op jit(solution)/shard_map/all_gather | solution.py:75
  84.8 2.8 %convolution_convert_fusion.1 = bf16[1536,512]{0,1:T(8,128)(2,1)} fusion(bf16[1536,256]{1,0:T(8,128)(2,1)S(1)} %all_gather.3, bf16[256,512]{1,0:T(8,128)(2,1)} %param.22), kind=kOutput, calls=%fused_computation.15 | convolution fusion | flops 403439616 | bytes 2621440 | tf_op jit(solution)/shard_map/dot_general | solution.py:77
  87.6 6.4 %fusion.4 = f32[512,1024]{1,0:T(8,128)} fusion(bf16[512,2048]{1,0:T(8,128)(2,1)} %bitcast.26, bf16[1,2048,1024]{2,1,0:T(8,128)(2,1)} %param.29), kind=kOutput, calls=%fused_computation.9 | convolution fusion | flops 2147483648 | bytes 8388608 | tf_op jit(solution)/shard_map/dot_general | solution.py:139
  94.0 10.5 %fusion.11 = bf16[2048,512]{0,1:T(8,128)(2,1)} fusion(bf16[1,1024,2048]{2,1,0:T(8,128)(2,1)} %param.31, f32[512,1024]{1,0:T(8,128)} %fusion.4, bf16[512,2048]{1,0:T(8,128)(2,1)} %bitcast.26, bf16[1,2048,1024]{2,1,0:T(8,128)(2,1)} %param.30), kind=kOutput, calls=%fused_computation.16 | convolution fusion | flops 4299161600 | bytes 14680064 | tf_op jit(solution)/shard_map/dot_general | solution.py:143
  106.3 2.7 %convolution_convert_fusion = bf16[1536,512]{0,1:T(8,128)(2,1)} fusion(bf16[1536,256]{1,0:T(8,128)(2,1)S(1)} %all_gather.3, bf16[256,512]{1,0:T(8,128)(2,1)} %param.23), kind=kOutput, calls=%fused_computation.14 | convolution fusion | flops 403439616 | bytes 2621440 | tf_op jit(solution)/shard_map/dot_general | solution.py:79
  109.8 3.2 %collective-permute-start.5 = (bf16[192,64]{0,1:T(8,128)(2,1)}, bf16[192,64]{0,1:T(8,128)(2,1)S(1)}, u32[]{:S(2)}, u32[]{:S(2)}) collective-permute-start(bf16[192,64]{0,1:T(8,128)(2,1)} %collective-permute-done.4), channel_id=1, source_target_pairs={{0,28},{4,0},{8,4},{12,8},{16,12},{20,16},{24,20},{28,24},{1,29},{... | collective-permute-start | bytes 73736 | tf_op jit(solution)/shard_map/ppermute | solution.py:30
  113.0 2.0 %convolution_bitcast_fusion.2 = f32[4,192,192]{2,1,0:T(8,128)} fusion(bf16[192,64]{0,1:T(8,128)(2,1)} %collective-permute-done.4, bf16[192,4,32]{0,2,1:T(8,128)(2,1)S(1)} %get-tuple-element.3, bf16[192,4,32]{0,2,1:T(8,128)(2,1)S(1)} %get-tuple-element.2), kind=kOutput, calls=%fused_computation.25 | convolution fusion | flops 19070976 | bytes 712704 | tf_op jit(solution)/shard_map/qhd,kd->hqk/dot_general | solution.py:86
  115.0 2.0 %convolution_bitcast_fusion.4 = f32[4,192,192]{2,1,0:T(8,128)} fusion(bf16[192,64]{0,1:T(8,128)(2,1)} %collective-permute-done, bf16[192,4,32]{0,2,1:T(8,128)(2,1)S(1)} %get-tuple-element.3, bf16[192,4,32]{0,2,1:T(8,128)(2,1)S(1)} %get-tuple-element.2), kind=kOutput, calls=%fused_computation.27 | convolution fusion | flops 19070976 | bytes 712704 | tf_op jit(solution)/shard_map/qhd,kd->hqk/dot_general | solution.py:86
  117.0 3.5 %collective-permute-start.6 = (bf16[192,64]{0,1:T(8,128)(2,1)S(1)}, bf16[192,64]{0,1:T(8,128)(2,1)S(1)}, u32[]{:S(2)}, u32[]{:S(2)}) collective-permute-start(bf16[192,64]{0,1:T(8,128)(2,1)S(1)} %collective-permute-done.5), channel_id=1, source_target_pairs={{0,28},{4,0},{8,4},{12,8},{16,12},{20,16},{24,20},{28,24},{1,29},{... | collective-permute-start | bytes 73736 | tf_op jit(solution)/shard_map/ppermute | solution.py:30
  121.7 1.2 convolution_bitcast_fusion.5
  125.4 2.7 %collective-permute-done.3 = bf16[192,64]{0,1:T(8,128)(2,1)S(1)} collective-permute-done((bf16[192,64]{0,1:T(8,128)(2,1)S(1)}, bf16[192,64]{0,1:T(8,128)(2,1)S(1)}, u32[]{:S(2)}, u32[]{:S(2)}) %collective-permute-start.3) | collective-permute-done | bytes 24608 | tf_op jit(solution)/shard_map/ppermute | solution.py:25
  129.3 12.7 %concatenate.19 = f32[4,192,3072]{2,1,0:T(8,128)} concatenate(f32[4,192,192]{2,1,0:T(8,128)} %convolution_bitcast_fusion.7, f32[4,192,192]{2,1,0:T(8,128)} %convolution_bitcast_fusion.6, f32[4,192,192]{2,1,0:T(8,128)} %convolution_bitcast_fusion.5, f32[4,192,192]{2,1,0:T(8,128)} %convolution_bitcast_fusion.4, f32[4,192,192]{2,1,0:T(8,128)S(1)} %convolution_bitcast_fusion.3, ...), dimensions={2} | concatenate | bytes 18874368 | tf_op jit(solution)/shard_map/jit(_roll_dynamic)/concatenate | solution.py:33
  142.0 4.4 %fusion.70 = (f32[4,192]{1,0:T(4,128)S(1)}, f32[4,192,1536]{2,1,0:T(8,128)S(1)}) fusion(f32[4,192,3072]{2,1,0:T(8,128)} %concatenate.19, s32[]{:T(128)S(6)} %select_n.44, bf16[1536,4,128]{0,2,1:T(8,128)(2,1)} %bitcast.114, bf16[192,4,128]{2,1,0:T(4,128)(2,1)S(1)} %slice-done), kind=kOutput, calls=%fused_computation.107 | convolution fusion | flops 305528064 | bytes 11209732 | tf_op jit(solution)/shard_map/qhd,khd->hqk/dot_general | solution.py:81
  148.8 1.5 convolution_convert_fusion.2
  150.3 3.5 %all-to-all-start.1 = ((bf16[512,8,64]{0,2,1:T(8,128)(2,1)}), bf16[512,8,64]{0,2,1:T(8,128)(2,1)S(1)}, u32[]{:S(2)}, u32[]{:S(2)}) async-start(bf16[512,8,64]{0,2,1:T(8,128)(2,1)} %bitcast.117), calls=%async_computation.3 | async-start | bytes 1048576 | tf_op jit(solution)/shard_map/all_to_all | solution.py:151
  154.4 14.7 %all-to-all-done.1 = bf16[512,8,64]{0,2,1:T(8,128)(2,1)S(1)} async-done(((bf16[512,8,64]{0,2,1:T(8,128)(2,1)}), bf16[512,8,64]{0,2,1:T(8,128)(2,1)S(1)}, u32[]{:S(2)}, u32[]{:S(2)}) %all-to-all-start.1) | async-done | bytes 524320 | tf_op jit(solution)/shard_map/all_to_all | solution.py:151
  170.4 1.5 multiply_reduce_fusion
  171.9 3.3 %reduce-scatter.3.cloned.1.call-done = bf16[48,2048]{1,0:T(8,128)(2,1)} async-done(((bf16[192,2048]{1,0:T(8,128)(2,1)}), bf16[48,2048]{1,0:T(8,128)(2,1)}) %reduce-scatter.3.cloned.1.call-update) | async-done | bytes 196624 | tf_op jit(solution)/shard_map/reduce_scatter | solution.py:102
  (99 shorter events, 19.8 us)
Async XLA Ops:
  7.2 141.6 %copy-start = (bf16[512,2048]{1,0:T(8,128)(2,1)S(1)}, bf16[512,2048]{1,0:T(8,128)(2,1)}, u32[]{:S(2)}) copy-start(bf16[512,2048]{1,0:T(8,128)(2,1)} %param.24) | copy-start | bytes 6291460
  19.0 6.6 %copy-start.8 = (bf16[192,64]{0,1:T(8,128)(2,1)S(1)}, bf16[192,64]{0,1:T(8,128)(2,1)}, u32[]{:S(2)}) copy-start(bf16[192,64]{0,1:T(8,128)(2,1)} %param.18) | copy-start | bytes 73732
  19.0 11.6 %copy-start.4 = (bf16[192,512]{1,0:T(8,128)(2,1)S(1)}, bf16[192,512]{1,0:T(8,128)(2,1)}, u32[]{:S(2)}) copy-start(bf16[192,512]{1,0:T(8,128)(2,1)} %param.16) | copy-start | bytes 589828
  19.0 11.8 %copy-start.3 = (bf16[512,768]{1,0:T(8,128)(2,1)S(1)}, bf16[512,768]{1,0:T(8,128)(2,1)}, u32[]{:S(2)}) copy-start(bf16[512,768]{1,0:T(8,128)(2,1)} %param.21) | copy-start | bytes 2359300
  19.0 11.8 %copy-start.11 = (f32[512]{0:T(512)S(1)}, f32[512]{0:T(512)}, u32[]{:S(2)}) copy-start(f32[512]{0:T(512)} %param.19) | copy-start | bytes 6148
  19.0 68.5 %all-to-all-start = ((bf16[8,64,2048]{2,1,0:T(8,128)(2,1)}), bf16[8,64,2048]{2,1,0:T(8,128)(2,1)}, u32[]{:S(2)}, u32[]{:S(2)}) async-start(bf16[8,64,2048]{2,1,0:T(8,128)(2,1)} %bitcast.113), calls=%async_computation.1 | async-start | bytes 4194304 | tf_op jit(solution)/shard_map/all_to_all | solution.py:136
  25.5 7.0 %copy-start.5 = (bf16[192,256]{1,0:T(8,128)(2,1)S(1)}, bf16[192,256]{1,0:T(8,128)(2,1)}, u32[]{:S(2)}) copy-start(bf16[192,256]{1,0:T(8,128)(2,1)} %param.17) | copy-start | bytes 294916
  25.5 7.1 %copy-start.12 = (f32[256]{0:T(256)S(1)}, f32[256]{0:T(256)}, u32[]{:S(2)}) copy-start(f32[256]{0:T(256)} %param.20) | copy-start | bytes 3076
  25.6 124.8 %reduce-scatter.5.cloned.1.call-start = ((), (), s32[]{:S(2)}) async-start(), calls=%async_computation.5 | async-start | bytes 2621440 | tf_op jit(solution)/shard_map/reduce_scatter | solution.py:142
  27.1 82.3 %collective-permute-start = (bf16[192,64]{0,1:T(8,128)(2,1)}, bf16[192,64]{0,1:T(8,128)(2,1)}, u32[]{:S(2)}, u32[]{:S(2)}) collective-permute-start(bf16[192,64]{0,1:T(8,128)(2,1)} %pad_maximum_fusion.1), channel_id=1, source_target_pairs={{0,4},{4,8},{8,12},{12,16},{16,20},{20,24},{24,28},{28,0},{1,5},{5... | collective-permute-start | bytes 73736 | tf_op jit(solution)/shard_map/ppermute | solution.py:25
  27.6 82.2 %collective-permute-start.4 = (bf16[192,64]{0,1:T(8,128)(2,1)}, bf16[192,64]{0,1:T(8,128)(2,1)}, u32[]{:S(2)}, u32[]{:S(2)}) collective-permute-start(bf16[192,64]{0,1:T(8,128)(2,1)} %pad_maximum_fusion.1), channel_id=1, source_target_pairs={{0,28},{4,0},{8,4},{12,8},{16,12},{20,16},{24,20},{28,24},{1,29},{... | collective-permute-start | bytes 73736 | tf_op jit(solution)/shard_map/ppermute | solution.py:30
  31.5 77.9 %copy-start.2 = (bf16[192,4,192]{2,1,0:T(4,128)(2,1)}, bf16[192,4,192]{2,1,0:T(4,128)(2,1)S(1)}, u32[]{:S(2)}) copy-start(bf16[192,4,192]{2,1,0:T(4,128)(2,1)S(1)} %reshape.186) | copy-start | bytes 884740
  104.6 0.8 copy-start.7
  104.6 70.6 %reduce-scatter.3.cloned.1.call-start = ((), (), s32[]{:S(2)}) async-start(), calls=%async_computation.4 | async-start | bytes 983040 | tf_op jit(solution)/shard_map/reduce_scatter | solution.py:102
  109.4 7.6 %collective-permute-start.1 = (bf16[192,64]{0,1:T(8,128)(2,1)}, bf16[192,64]{0,1:T(8,128)(2,1)S(1)}, u32[]{:S(2)}, u32[]{:S(2)}) collective-permute-start(bf16[192,64]{0,1:T(8,128)(2,1)} %collective-permute-done), channel_id=1, source_target_pairs={{0,4},{4,8},{8,12},{12,16},{16,20},{20,24},{24,28},{28,0},{1,5},{5... | collective-permute-start | bytes 73736 | tf_op jit(solution)/shard_map/ppermute | solution.py:25
  109.8 7.2 %collective-permute-start.5 = (bf16[192,64]{0,1:T(8,128)(2,1)}, bf16[192,64]{0,1:T(8,128)(2,1)S(1)}, u32[]{:S(2)}, u32[]{:S(2)}) collective-permute-start(bf16[192,64]{0,1:T(8,128)(2,1)} %collective-permute-done.4), channel_id=1, source_target_pairs={{0,28},{4,0},{8,4},{12,8},{16,12},{20,16},{24,20},{28,24},{1,29},{... | collective-permute-start | bytes 73736 | tf_op jit(solution)/shard_map/ppermute | solution.py:30
  117.0 6.0 %collective-permute-start.2 = (bf16[192,64]{0,1:T(8,128)(2,1)S(1)}, bf16[192,64]{0,1:T(8,128)(2,1)S(1)}, u32[]{:S(2)}, u32[]{:S(2)}) collective-permute-start(bf16[192,64]{0,1:T(8,128)(2,1)S(1)} %collective-permute-done.1), channel_id=1, source_target_pairs={{0,4},{4,8},{8,12},{12,16},{16,20},{20,24},{24,28},{28,0},{1,5},{5... | collective-permute-start | bytes 73736 | tf_op jit(solution)/shard_map/ppermute | solution.py:25
  117.0 7.2 %collective-permute-start.6 = (bf16[192,64]{0,1:T(8,128)(2,1)S(1)}, bf16[192,64]{0,1:T(8,128)(2,1)S(1)}, u32[]{:S(2)}, u32[]{:S(2)}) collective-permute-start(bf16[192,64]{0,1:T(8,128)(2,1)S(1)} %collective-permute-done.5), channel_id=1, source_target_pairs={{0,28},{4,0},{8,4},{12,8},{16,12},{20,16},{24,20},{28,24},{1,29},{... | collective-permute-start | bytes 73736 | tf_op jit(solution)/shard_map/ppermute | solution.py:30
  123.0 5.1 %collective-permute-start.3 = (bf16[192,64]{0,1:T(8,128)(2,1)S(1)}, bf16[192,64]{0,1:T(8,128)(2,1)S(1)}, u32[]{:S(2)}, u32[]{:S(2)}) collective-permute-start(bf16[192,64]{0,1:T(8,128)(2,1)S(1)} %collective-permute-done.2), channel_id=1, source_target_pairs={{0,4},{4,8},{8,12},{12,16},{16,20},{20,24},{24,28},{28,0},{1,5},{5... | collective-permute-start | bytes 73736 | tf_op jit(solution)/shard_map/ppermute | solution.py:25
  129.3 12.7 %slice-start = ((bf16[192,4,192]{2,1,0:T(4,128)(2,1)}), bf16[192,4,128]{2,1,0:T(4,128)(2,1)S(1)}, s32[]{:S(2)}) async-start(bf16[192,4,192]{2,1,0:T(4,128)(2,1)} %copy-done.2), calls=%async_computation.6 | async-start | bytes 393216 | tf_op jit(solution)/shard_map/slice | solution.py:67
  146.5 1.4 copy-start.1
  148.8 5.3 %copy-start.9 = (s32[128,2]{0,1:T(2,128)S(1)}, s32[128,2]{0,1:T(2,128)}, u32[]{:S(2)}) copy-start(s32[128,2]{0,1:T(2,128)} %param.27) | copy-start | bytes 3076
  148.8 5.4 %copy-start.10 = (f32[128,2]{0,1:T(2,128)S(1)}, f32[128,2]{0,1:T(2,128)}, u32[]{:S(2)}) copy-start(f32[128,2]{0,1:T(2,128)} %param.28) | copy-start | bytes 3076
  150.3 18.8 %all-to-all-start.1 = ((bf16[512,8,64]{0,2,1:T(8,128)(2,1)}), bf16[512,8,64]{0,2,1:T(8,128)(2,1)S(1)}, u32[]{:S(2)}, u32[]{:S(2)}) async-start(bf16[512,8,64]{0,2,1:T(8,128)(2,1)} %bitcast.117), calls=%async_computation.3 | async-start | bytes 1048576 | tf_op jit(solution)/shard_map/all_to_all | solution.py:151
  (1 other events, 0.8 us)
Sparse Core Ops, SparseCore 0:
  104.7 35.5 reduce-scatter.4
  150.4 24.6 reduce-scatter.2
